TPU v7x, 512 devices: a whole 4x8x8 slice. The times are simulated.
512 devices in a mesh: sp: 64 (over z, y), tp: 8 (over x, core).
Axes of the slice: x: 4, y: 8, z: 8, core: 2. Of those that a mesh axis runs over, the one named last changes fastest.
Arguments:
- latent: bfloat16 [16384, 2048], P(('sp', 'tp')), may hold values from -6 to 6
- context: bfloat16 [512, 2048], P('sp'), may hold values from -6 to 6
- condition: float32 [2048], P('tp'), may hold values from -6 to 6
- context_condition: float32 [2048], P('tp'), may hold values from -6 to 6
- modulation_weight: bfloat16 [2048, 6144], P('tp', 'sp'), may hold values from -0.125 to 0.125
- query_first: bfloat16 [2048, 512], P(None, 'tp'), may hold values from -1 to 1
- query_second: bfloat16 [2048, 512], P(None, 'tp'), may hold values from -1 to 1
- key_first: bfloat16 [2048, 512], P(None, 'tp'), may hold values from -1 to 1
- key_second: bfloat16 [2048, 512], P(None, 'tp'), may hold values from -1 to 1
- value_weight: bfloat16 [2048, 1024], P(None, 'tp'), may hold values from -0.125 to 0.125
- lambda_head: float32 [8], P('tp'), may hold values from 0.3 to 0.8
- context_score_boost: float32 [8], P('tp'), may hold values from 1.5 to 3
- head_gain: float32 [128], replicated, may hold values from 0.1 to 1.9
- output_weight: bfloat16 [1024, 2048], P('tp'), may hold values from -0.1875 to 0.1875
Outputs:
- updated: bfloat16 [16384, 2048], P(('sp', 'tp'))
All inputs are finite; a program needn't handle non-finite values.
Results may differ from a plain program's by a relative error of at most 0.0095.
Values may be sent and summed in bfloat16 or wider, within the bound.
A program may use at most 64 MiB of HBM per device.

v0:
```python
import jax
import jax.numpy as jnp
from jax import lax
from jax.sharding import PartitionSpec as P

HEAD_DIM = 64
VALUE_DIM = 128
GRID_W = 64
EPSILON = 1e-06
THETA = 10000.0
NEGATIVE = -1e30


def copy_for_each(shard, axis):
    size = lax.axis_size(axis)
    return lax.all_to_all(
        jnp.broadcast_to(shard[None], (size, *shard.shape)), axis, 0, 0, tiled=True
    )


def taken_together(shard, axis):
    return copy_for_each(shard, axis).sum(axis=0)


def joined_along(tiles, dim):
    tiles = jnp.moveaxis(tiles, 0, dim)
    lengths = tiles.shape
    return tiles.reshape(*lengths[:dim], lengths[dim] * lengths[dim + 1], *lengths[dim + 2 :])


def collect(shard, axis, dim):
    return joined_along(copy_for_each(shard, axis), dim)


def in_one_piece(arrays, axis, dim, along):
    widths = [a.shape[along] for a in arrays]
    both = jnp.concatenate(arrays, axis=along)
    out = lax.all_gather(both, axis, axis=dim, tiled=True)
    return tuple(jnp.split(out, [sum(widths[:k]) for k in range(1, len(widths))], axis=along))


def in_blocks(shard, dim, size):
    before, after = (shard.shape[:dim], shard.shape[dim + 1 :])
    return jnp.moveaxis(shard.reshape(*before, size, -1, *after), dim, 0)


def sum_at_owner(shard, axis, dim):
    tiles = in_blocks(shard, dim, lax.axis_size(axis))
    arrived = lax.all_to_all(tiles, axis, split_axis=0, concat_axis=0, tiled=True)
    return arrived.astype(jnp.float32).sum(axis=0)


def norm_rows(rows):
    values = rows.astype(jnp.float32)
    return values * lax.rsqrt(jnp.mean(values * values, axis=-1, keepdims=True) + EPSILON)


def rotate_pairs(values, positions):
    half = values.shape[-1] // 2
    quarter = half // 2
    reciprocal_norm = THETA ** (-jnp.arange(quarter, dtype=jnp.float32) / quarter)

    def turn(part, where):
        angle = where.astype(jnp.float32)[:, None] * reciprocal_norm[None, :]
        cosine_table = jnp.concatenate([jnp.cos(angle)] * 2, -1)[:, None, :]
        sine = jnp.concatenate([jnp.sin(angle)] * 2, -1)[:, None, :]
        flipped = jnp.concatenate([-part[..., quarter:], part[..., :quarter]], -1)
        return part * cosine_table + flipped * sine

    grid_row = positions // GRID_W
    grid_col = positions % GRID_W
    return jnp.concatenate(
        [turn(values[..., :half], grid_row), turn(values[..., half:], grid_col)], -1
    )


def block_extent(rows):
    size = min(rows, 1024)
    while rows % size:
        size -= 1
    return size


def body(
    latent,
    context,
    condition,
    context_condition,
    modulation_weight,
    query_first,
    query_second,
    key_first,
    key_second,
    value_weight,
    lambda_head,
    context_score_boost,
    head_gain,
    output_weight,
):
    width = latent.shape[1]
    signal = jax.nn.silu(jnp.stack([condition, context_condition])).astype(jnp.bfloat16)
    partial_mod = jnp.dot(signal, modulation_weight, preferred_element_type=jnp.float32)
    reduced = taken_together(partial_mod, "tp")
    modulation = collect(reduced, "sp", 1)
    shift = modulation[:, :width]
    scale = modulation[:, width : 2 * width]
    gate = modulation[:, 2 * width :]
    h_latent = (norm_rows(latent) * (1.0 + scale[0]) + shift[0]).astype(jnp.bfloat16)
    h_context = (norm_rows(context) * (1.0 + scale[1]) + shift[1]).astype(jnp.bfloat16)
    heads_dev = value_weight.shape[1] // VALUE_DIM
    span = heads_dev * HEAD_DIM
    offset = lax.axis_index("sp") * (latent.shape[0] * lax.axis_size("tp"))
    piece = collect(h_latent, "tp", 0)
    count = piece.shape[0]
    positions = offset + jnp.arange(count, dtype=jnp.int32)
    turned = []
    for weight in (query_first, query_second, key_first, key_second):
        product = jnp.dot(piece, weight, preferred_element_type=jnp.float32).reshape(
            count, heads_dev, HEAD_DIM
        )
        turned.append(rotate_pairs(product, positions).astype(jnp.bfloat16).reshape(count, span))
    values = jnp.dot(piece, value_weight, preferred_element_type=jnp.float32).astype(jnp.bfloat16)
    projected = jnp.concatenate(turned + [values], axis=1)
    queries = projected.shape[0]
    queries_one = projected[:, :span].reshape(queries, heads_dev, HEAD_DIM)
    queries_two = projected[:, span : 2 * span].reshape(queries, heads_dev, HEAD_DIM)
    latent_keys = projected[:, 2 * span : 4 * span]
    latent_values = projected[:, 4 * span :]

    def update(carry, block):
        keys_pair, values, boolean_markers = block
        count = keys_pair.shape[0]
        keys_one = keys_pair[:, :span].reshape(count, heads_dev, HEAD_DIM)
        keys_two = keys_pair[:, span:].reshape(count, heads_dev, HEAD_DIM)
        values_heads = values.reshape(count, heads_dev, VALUE_DIM)
        extra_score = context_score_boost[:, None, None] * boolean_markers[None, None, :]
        renewed = []
        for (highest, totals, weighted), query, keys in zip(
            carry, (queries_one, queries_two), (keys_one, keys_two)
        ):
            scores = (
                jnp.einsum("qhd,khd->hqk", query, keys, preferred_element_type=jnp.float32)
                * HEAD_DIM ** (-0.5)
                + extra_score
            )
            peak = jnp.maximum(highest, jnp.max(scores, axis=-1))
            exp_weights = jnp.exp(scores - peak[..., None])
            rescale = jnp.exp(highest - peak)
            totals = totals * rescale + jnp.sum(exp_weights, axis=-1)
            weighted = weighted * jnp.transpose(rescale)[:, :, None] + jnp.einsum(
                "hqk,khe->qhe",
                exp_weights.astype(jnp.bfloat16),
                values_heads,
                preferred_element_type=jnp.float32,
            )
            renewed.append((peak, totals, weighted))
        return (tuple(renewed), None)

    def fold_keys(carry, keys_pair, values, boolean_markers):
        rows = keys_pair.shape[0]
        size = block_extent(rows)
        count = rows // size
        blocks = (
            keys_pair.reshape(count, size, keys_pair.shape[1]),
            values.reshape(count, size, values.shape[1]),
            boolean_markers.reshape(count, size),
        )
        carry, unused = lax.scan(update, carry, blocks)
        return carry

    start_state = (
        jnp.full((heads_dev, queries), NEGATIVE, jnp.float32),
        jnp.zeros((heads_dev, queries), jnp.float32),
        jnp.zeros((queries, heads_dev, VALUE_DIM), jnp.float32),
    )
    initial = (start_state, start_state)
    keys_pair = jnp.concatenate(
        [
            jnp.dot(h_context, key_first, preferred_element_type=jnp.float32).astype(jnp.bfloat16),
            jnp.dot(h_context, key_second, preferred_element_type=jnp.float32).astype(jnp.bfloat16),
        ],
        axis=1,
    )
    values = jnp.dot(h_context, value_weight, preferred_element_type=jnp.float32).astype(
        jnp.bfloat16
    )
    all_keys, all_values = in_one_piece((keys_pair, values), "sp", 0, 1)
    carry = fold_keys(initial, all_keys, all_values, jnp.ones((all_keys.shape[0],), jnp.float32))
    pieces = (
        lax.all_gather(latent_keys, "sp", axis=0, tiled=True),
        lax.all_gather(latent_values, "sp", axis=0, tiled=True),
    )
    boolean_markers = jnp.zeros((pieces[0].shape[0],), jnp.float32)
    final = fold_keys(carry, pieces[0], pieces[1], boolean_markers)
    outcomes = [weighted / jnp.transpose(totals)[:, :, None] for highest, totals, weighted in final]
    mixed = outcomes[0] - lambda_head[None, :, None] * outcomes[1]
    normed = (
        mixed * lax.rsqrt(jnp.mean(mixed * mixed, axis=-1, keepdims=True) + EPSILON) * head_gain
    )
    heads_out = normed.astype(jnp.bfloat16).reshape(queries, heads_dev * VALUE_DIM)
    branch = sum_at_owner(
        jnp.dot(heads_out, output_weight, preferred_element_type=jnp.float32).astype(jnp.bfloat16),
        "tp",
        0,
    )
    return (latent.astype(jnp.float32) + gate[0] * branch).astype(jnp.bfloat16)


def solution(mesh):
    in_specs = (
        P(("sp", "tp"), None),
        P("sp", None),
        P("tp"),
        P("tp"),
        P("tp", "sp"),
        P(None, "tp"),
        P(None, "tp"),
        P(None, "tp"),
        P(None, "tp"),
        P(None, "tp"),
        P("tp"),
        P("tp"),
        P(),
        P("tp", None),
    )
    out_specs = P(("sp", "tp"), None)
    return jax.shard_map(body, mesh=mesh, in_specs=in_specs, out_specs=out_specs, check_vma=False)
```

profile of v0, /device:TPU:1, one launch (start us, length us, event | category | flops | bytes accessed | tf_op | source)
XLA Modules:
  0.0 344.7 jit_solution(9492942217073333725)
XLA Ops:
  6.5 1.1 fusion.88
  8.2 10.1 %all-to-all-start = ((f32[8,2,96]{2,1,0:T(2,128)}), f32[8,2,96]{2,1,0:T(2,128)S(1)}, u32[]{:S(2)}, u32[]{:S(2)}) async-start(f32[8,2,96]{2,1,0:T(2,128)} %broadcast_in_dim.22), calls=%async_computation | async-start | bytes 16384 | tf_op jit(solution)/shard_map/all_to_all | solution.py:16
  18.3 1.0 fusion.32
  19.3 3.6 %all-to-all-done = f32[8,2,96]{2,1,0:T(2,128)S(1)} async-done(((f32[8,2,96]{2,1,0:T(2,128)}), f32[8,2,96]{2,1,0:T(2,128)S(1)}, u32[]{:S(2)}, u32[]{:S(2)}) %all-to-all-start) | async-done | bytes 6176 | tf_op jit(solution)/shard_map/all_to_all | solution.py:16
  23.6 12.0 %all-to-all-start.1 = ((f32[64,2,96]{2,1,0:T(2,128)}), f32[64,2,96]{2,1,0:T(2,128)S(1)}, u32[]{:S(2)}, u32[]{:S(2)}) async-start(f32[64,2,96]{2,1,0:T(2,128)} %broadcast_in_dim.23), calls=%async_computation.1 | async-start | bytes 131072 | tf_op jit(solution)/shard_map/all_to_all | solution.py:16
  35.6 11.1 %all-to-all-done.1 = f32[64,2,96]{2,1,0:T(2,128)S(1)} async-done(((f32[64,2,96]{2,1,0:T(2,128)}), f32[64,2,96]{2,1,0:T(2,128)S(1)}, u32[]{:S(2)}, u32[]{:S(2)}) %all-to-all-start.1) | async-done | bytes 49184 | tf_op jit(solution)/shard_map/all_to_all | solution.py:16
  46.9 1.0 fusion.35
  47.9 1.1 broadcast_in_dim.25
  49.0 5.7 %all-to-all-start.2 = ((bf16[8,32,2048]{2,1,0:T(8,128)(2,1)}), bf16[8,32,2048]{2,1,0:T(8,128)(2,1)S(1)}, u32[]{:S(2)}, u32[]{:S(2)}) async-start(bf16[8,32,2048]{2,1,0:T(8,128)(2,1)} %broadcast_in_dim.25), calls=%async_computation.2 | async-start | bytes 2097152 | tf_op jit(solution)/shard_map/all_to_all | solution.py:16
  55.0 14.8 %all-to-all-done.2 = bf16[8,32,2048]{2,1,0:T(8,128)(2,1)S(1)} async-done(((bf16[8,32,2048]{2,1,0:T(8,128)(2,1)}), bf16[8,32,2048]{2,1,0:T(8,128)(2,1)S(1)}, u32[]{:S(2)}, u32[]{:S(2)}) %all-to-all-start.2) | async-done | bytes 1048608 | tf_op jit(solution)/shard_map/all_to_all | solution.py:16
  71.4 1.1 convolution_convert_fusion.1
  74.8 35.7 %all_gather.9 = bf16[512,256]{1,0:T(8,128)(2,1)S(1)} all-gather(bf16[8,256]{1,0:T(8,128)(2,1)S(1)} %pad_maximum_fusion.5), channel_id=1, replica_groups=mesh['sp'=64,'tp'=8] {'sp'}, dimensions={0}, use_global_device_ids=true | all-gather | bytes 266240 | tf_op jit(solution)/shard_map/all_gather | solution.py:38
  113.4 35.7 %all-gather.3.cloned.1.call-done = bf16[16384,128]{0,1:T(8,128)(2,1)} async-done(((bf16[256,128]{0,1:T(8,128)(2,1)}), bf16[16384,128]{0,1:T(8,128)(2,1)}) %all-gather.3.cloned.1.call-update) | async-done | bytes 4194320 | tf_op jit(solution)/shard_map/all_gather | solution.py:190
  149.0 6.4 %copy.26 = bf16[16384,128]{1,0:T(8,128)(2,1)} copy(bf16[16384,128]{0,1:T(8,128)(2,1)} %all-gather.3.cloned.1.call-done) | data formatting | bytes 8388608 | tf_op jit(solution)/shard_map/while | solution.py:168
  155.4 79.0 %all-gather.5.cloned.1.call-done = bf16[16384,128]{1,0:T(8,128)(2,1)} async-done(((bf16[256,128]{1,0:T(8,128)(2,1)}), bf16[16384,128]{1,0:T(8,128)(2,1)}) %all-gather.5.cloned.1.call-update) | async-done | bytes 4194320 | tf_op jit(solution)/shard_map/all_gather | solution.py:191
  234.5 78.2 %while.4 = (s32[]{:T(128)}, f32[1,256]{1,0:T(1,128)S(1)}, f32[1,256]{1,0:T(1,128)S(1)}, f32[256,1,128]{0,2,1:T(8,128)S(1)}, f32[1,256]{1,0:T(1,128)S(1)}, /*inde...) while((s32[]{:T(128)}, f32[1,256]{1,0:T(1,128)S(1)}, ...), condition=%wide.region_12.13_spmd, body=%wide.region_7.12_spmd.sunk | while | flops 205128704 | bytes 8488073 | solution.py:168
  234.5 1.0 dynamic-slice_bitcast_fusion.2
  236.6 1.3 fusion.140
  238.0 1.3 fusion.139
  239.4 1.0 dynamic-slice_bitcast_fusion.2
  241.5 1.3 fusion.140
  242.9 1.3 fusion.139
  244.2 1.0 dynamic-slice_bitcast_fusion.2
  246.4 1.3 fusion.140
  247.8 1.3 fusion.139
  249.1 1.0 dynamic-slice_bitcast_fusion.2
  251.3 1.3 fusion.140
  252.6 1.3 fusion.139
  254.0 1.0 dynamic-slice_bitcast_fusion.2
  256.2 1.3 fusion.140
  257.5 1.3 fusion.139
  258.9 1.0 dynamic-slice_bitcast_fusion.2
  261.1 1.3 fusion.140
  262.4 1.3 fusion.139
  263.8 1.0 dynamic-slice_bitcast_fusion.2
  266.0 1.3 fusion.140
  267.3 1.3 fusion.139
  268.7 1.0 dynamic-slice_bitcast_fusion.2
  270.8 1.3 fusion.140
  272.2 1.3 fusion.139
  273.5 1.0 dynamic-slice_bitcast_fusion.2
  275.7 1.3 fusion.140
  277.1 1.3 fusion.139
  278.4 1.0 dynamic-slice_bitcast_fusion.2
  280.6 1.3 fusion.140
  281.9 1.3 fusion.139
  283.3 1.0 dynamic-slice_bitcast_fusion.2
  285.5 1.3 fusion.140
  286.8 1.3 fusion.139
  288.2 1.0 dynamic-slice_bitcast_fusion.2
  290.4 1.3 fusion.140
  291.7 1.3 fusion.139
  293.1 1.0 dynamic-slice_bitcast_fusion.2
  295.3 1.3 fusion.140
  296.6 1.3 fusion.139
  300.1 1.3 fusion.140
  301.5 1.3 fusion.139
  302.9 1.0 dynamic-slice_bitcast_fusion.2
  305.0 1.3 fusion.140
  306.4 1.3 fusion.139
  307.7 1.0 dynamic-slice_bitcast_fusion.2
  309.9 1.3 fusion.140
  311.2 1.3 fusion.139
  313.2 23.8 %all_to_all.20 = bf16[8,32,2048]{2,1,0:T(8,128)(2,1)S(1)} all-to-all(bf16[8,32,2048]{2,1,0:T(8,128)(2,1)S(1)} %bitcast.183), channel_id=1, replica_groups=mesh['sp'=64,'tp'=8] {'tp'}, dimensions={0} | all-to-all | bytes 2097152 | tf_op jit(solution)/shard_map/all_to_all | solution.py:49
  (213 shorter events, 28.4 us)
Async XLA Ops:
  6.5 306.2 %copy-start = (bf16[128,2048]{1,0:T(8,128)(2,1)S(1)}, bf16[128,2048]{1,0:T(8,128)(2,1)}, u32[]{:S(2)}) copy-start(bf16[128,2048]{1,0:T(8,128)(2,1)} %param.29) | copy-start | bytes 1572868
  6.5 63.2 %copy-start.3 = (bf16[2048,64]{0,1:T(8,128)(2,1)S(1)}, bf16[2048,64]{0,1:T(8,128)(2,1)}, u32[]{:S(2)}) copy-start(bf16[2048,64]{0,1:T(8,128)(2,1)} %param.23) | copy-start | bytes 786436
  6.5 63.7 %copy-start.4 = (bf16[2048,64]{0,1:T(8,128)(2,1)S(1)}, bf16[2048,64]{0,1:T(8,128)(2,1)}, u32[]{:S(2)}) copy-start(bf16[2048,64]{0,1:T(8,128)(2,1)} %param.24) | copy-start | bytes 786436
  6.5 64.9 %copy-start.1 = (bf16[2048,128]{1,0:T(8,128)(2,1)S(1)}, bf16[2048,128]{1,0:T(8,128)(2,1)}, u32[]{:S(2)}) copy-start(bf16[2048,128]{1,0:T(8,128)(2,1)} %param.25) | copy-start | bytes 1572868
  8.2 14.7 %all-to-all-start = ((f32[8,2,96]{2,1,0:T(2,128)}), f32[8,2,96]{2,1,0:T(2,128)S(1)}, u32[]{:S(2)}, u32[]{:S(2)}) async-start(f32[8,2,96]{2,1,0:T(2,128)} %broadcast_in_dim.22), calls=%async_computation | async-start | bytes 16384 | tf_op jit(solution)/shard_map/all_to_all | solution.py:16
  23.6 23.1 %all-to-all-start.1 = ((f32[64,2,96]{2,1,0:T(2,128)}), f32[64,2,96]{2,1,0:T(2,128)S(1)}, u32[]{:S(2)}, u32[]{:S(2)}) async-start(f32[64,2,96]{2,1,0:T(2,128)} %broadcast_in_dim.23), calls=%async_computation.1 | async-start | bytes 131072 | tf_op jit(solution)/shard_map/all_to_all | solution.py:16
  47.9 25.9 %copy-start.7 = (bf16[8,2048]{1,0:T(8,128)(2,1)S(1)}, bf16[8,2048]{1,0:T(8,128)(2,1)}, u32[]{:S(2)}) copy-start(bf16[8,2048]{1,0:T(8,128)(2,1)} %param.17) | copy-start | bytes 98308
  49.0 61.5 %copy-start.5 = (bf16[2048,64]{0,1:T(8,128)(2,1)S(1)}, bf16[2048,64]{0,1:T(8,128)(2,1)}, u32[]{:S(2)}) copy-start(bf16[2048,64]{0,1:T(8,128)(2,1)} %param.22) | copy-start | bytes 786436
  49.0 20.7 %all-to-all-start.2 = ((bf16[8,32,2048]{2,1,0:T(8,128)(2,1)}), bf16[8,32,2048]{2,1,0:T(8,128)(2,1)S(1)}, u32[]{:S(2)}, u32[]{:S(2)}) async-start(bf16[8,32,2048]{2,1,0:T(8,128)(2,1)} %broadcast_in_dim.25), calls=%async_computation.2 | async-start | bytes 2097152 | tf_op jit(solution)/shard_map/all_to_all | solution.py:16
  54.7 94.3 %all-gather.3.cloned.1.call-start = ((), (), s32[]{:S(2)}) async-start(), calls=%async_computation.4 | async-start | bytes 4259840 | tf_op jit(solution)/shard_map/all_gather | solution.py:190
  69.7 41.2 %copy-start.6 = (bf16[2048,64]{0,1:T(8,128)(2,1)S(1)}, bf16[2048,64]{0,1:T(8,128)(2,1)}, u32[]{:S(2)}) copy-start(bf16[2048,64]{0,1:T(8,128)(2,1)} %param.21) | copy-start | bytes 786436
  71.4 163.1 %all-gather.5.cloned.1.call-start = ((), (), s32[]{:S(2)}) async-start(), calls=%async_computation.5 | async-start | bytes 4259840 | tf_op jit(solution)/shard_map/all_gather | solution.py:191
  234.5 78.2 %copy-start.8 = (f32[128]{0:T(128)S(1)}, f32[128]{0:T(128)}, u32[]{:S(2)}) copy-start(f32[128]{0:T(128)} %param.28) | copy-start | bytes 1540
  312.6 24.6 %copy-start.2 = (bf16[32,2048]{1,0:T(8,128)(2,1)S(1)}, bf16[32,2048]{1,0:T(8,128)(2,1)}, u32[]{:S(2)}) copy-start(bf16[32,2048]{1,0:T(8,128)(2,1)} %param.16) | copy-start | bytes 393220
Sparse Core Ops, SparseCore 0:
  71.5 77.4 all-gather.2
  152.1 82.3 all-gather.4
where the time goes:
time: 347 us; the launch traced here: 345 us
  waiting for transfers between devices  144 us (41%)
  matrix products  60.3 us (17%)
  blocking collectives  59.5 us (17%)
  starting transfers between devices  27.8 us (8%)
  local copies, waits for them, and re-layouts  24.6 us (7%)
  between operations  14.9 us (4%)
  other arithmetic  12.3 us (4%)
    all_gather x1, waiting for transfers between devices, body(): lax.all_gather(latent_values, 'sp', axis=0, tiled=True)  79 us
    dot_general x34, matrix products, update(): jnp.einsum('hqk,khe->qhe', exp_weights.astype(jnp.bfloat16), values_heads...  43.2 us
    all_gather x1, blocking collectives, in_one_piece(): out = lax.all_gather(both, axis, axis=dim, tiled=True)  35.7 us
    all_gather x1, waiting for transfers between devices, body(): lax.all_gather(latent_keys, 'sp', axis=0, tiled=True)  35.7 us
    all_to_all x3, waiting for transfers between devices, copy_for_each(): lax.all_to_all(jnp.broadcast_to(shard[None], (size, *shard.shape)), axis,...  29.4 us
    all_to_all x3, starting transfers between devices, copy_for_each(): lax.all_to_all(jnp.broadcast_to(shard[None], (size, *shard.shape)), axis,...  27.8 us
    all_to_all x1, blocking collectives, sum_at_owner(): lax.all_to_all(tiles, axis, split_axis=0, concat_axis=0, tiled=True)  23.8 us
    squeeze x16, local copies, waits for them, and re-layouts, fold_keys(): carry, unused = lax.scan(update, carry, blocks)  15.6 us
  transfers between devices with their start and end apart: 5, of which 5 were waited for; matrix products, arithmetic and copies ran while one was open for 4% of the time, Pallas kernels for 0%

commit v1 on v0

--- a/solution.py
+++ b/solution.py
@@ -9,6 +9,15 @@
 EPSILON = 1e-06
 THETA = 10000.0
 NEGATIVE = -1e30
+
+
+def record_meet(message):
+    fields = []
+    for _ in range(jax.lax.psum(1, "sp")):
+        fields.append(message)
+    taken_in = jnp.stack(fields, 0)
+    t_next = jax.lax.all_to_all(taken_in, "sp", 0, 0)
+    return jnp.concatenate(t_next, 0)
 
 
 def copy_for_each(shard, axis):
@@ -186,10 +195,7 @@
     )
     all_keys, all_values = in_one_piece((keys_pair, values), "sp", 0, 1)
     carry = fold_keys(initial, all_keys, all_values, jnp.ones((all_keys.shape[0],), jnp.float32))
-    pieces = (
-        lax.all_gather(latent_keys, "sp", axis=0, tiled=True),
-        lax.all_gather(latent_values, "sp", axis=0, tiled=True),
-    )
+    pieces = (lax.all_gather(latent_keys, "sp", axis=0, tiled=True), record_meet(latent_values))
     boolean_markers = jnp.zeros((pieces[0].shape[0],), jnp.float32)
     final = fold_keys(carry, pieces[0], pieces[1], boolean_markers)
     outcomes = [weighted / jnp.transpose(totals)[:, :, None] for highest, totals, weighted in final]

time: 347 us -> 371 us (1.069)
  blocking collectives: 59.5 us -> 186 us
  waiting for transfers between devices: 144 us -> 34.3 us
  starting transfers between devices: 27.8 us -> 33.5 us
    all_gather x1, blocking collectives: 35.7 us -> 161 us  [in_one_piece(): out = lax.all_gather(both, axis, axis=dim, tiled=True)]
    all_gather x1 -> x0, waiting for transfers between devices: 79 us -> none  [body(): lax.all_gather(latent_values, 'sp', axis=0, tiled=True)]
    all_gather x1, waiting for transfers between devices: 35.7 us -> 4.84 us  [body(): lax.all_gather(latent_keys, 'sp', axis=0, tiled=True)]
    all_to_all x0 -> x1, starting transfers between devices: none -> 5.79 us  [record_meet(): t_next = jax.lax.all_to_all(taken_in, 'sp', 0, 0)]
  transfers between devices with their start and end apart: 5 -> 5, of which waited for: 5 -> 4; matrix products, arithmetic and copies ran while one was open for 4% -> 4% of each run, Pallas kernels for 0% -> 0%
where the time goes in v1:
time: 371 us; the launch traced here: 369 us
  blocking collectives  186 us (50%)
  matrix products  59.7 us (16%)
  waiting for transfers between devices  34.3 us (9%)
  starting transfers between devices  33.5 us (9%)
  local copies, waits for them, and re-layouts  27.5 us (7%)
  between operations  14.9 us (4%)
  other arithmetic  12.3 us (3%)
    all_gather x1, blocking collectives, in_one_piece(): out = lax.all_gather(both, axis, axis=dim, tiled=True)  161 us
    dot_general x34, matrix products, update(): jnp.einsum('hqk,khe->qhe', exp_weights.astype(jnp.bfloat16), values_heads...  43.2 us
    all_to_all x3, waiting for transfers between devices, copy_for_each(): lax.all_to_all(jnp.broadcast_to(shard[None], (size, *shard.shape)), axis,...  29.4 us
    all_to_all x3, starting transfers between devices, copy_for_each(): lax.all_to_all(jnp.broadcast_to(shard[None], (size, *shard.shape)), axis,...  27.7 us
    all_to_all x1, blocking collectives, sum_at_owner(): lax.all_to_all(tiles, axis, split_axis=0, concat_axis=0, tiled=True)  25 us
    squeeze x16, local copies, waits for them, and re-layouts, fold_keys(): carry, unused = lax.scan(update, carry, blocks)  15.6 us
    dot_general x34, matrix products, update(): jnp.einsum('qhd,khd->hqk', query, keys, preferred_element_type=jnp.float32)  12 us
    reduce_sum x34, other arithmetic, update(): totals = totals * rescale + jnp.sum(exp_weights, axis=-1)  7.59 us
  transfers between devices with their start and end apart: 5, of which 4 were waited for; matrix products, arithmetic and copies ran while one was open for 4% of the time, Pallas kernels for 0%

profile of v1, /device:TPU:1, one launch (start us, length us, event | category | flops | bytes accessed | tf_op | source)
XLA Modules:
  0.0 368.9 jit_solution(741000447298736071)
XLA Ops:
  6.5 1.1 fusion.88
  8.2 10.1 %all-to-all-start = ((f32[8,2,96]{2,1,0:T(2,128)}), f32[8,2,96]{2,1,0:T(2,128)S(1)}, u32[]{:S(2)}, u32[]{:S(2)}) async-start(f32[8,2,96]{2,1,0:T(2,128)} %broadcast_in_dim.22), calls=%async_computation | async-start | bytes 16384 | tf_op jit(solution)/shard_map/all_to_all | solution.py:25
  18.3 1.0 fusion.32
  19.3 3.6 all-to-all-done
  23.6 12.0 %all-to-all-start.1 = ((f32[64,2,96]{2,1,0:T(2,128)}), f32[64,2,96]{2,1,0:T(2,128)S(1)}, u32[]{:S(2)}, u32[]{:S(2)}) async-start(f32[64,2,96]{2,1,0:T(2,128)} %broadcast_in_dim.23), calls=%async_computation.1 | async-start | bytes 131072 | tf_op jit(solution)/shard_map/all_to_all | solution.py:25
  35.6 11.1 %all-to-all-done.1 = f32[64,2,96]{2,1,0:T(2,128)S(1)} async-done(((f32[64,2,96]{2,1,0:T(2,128)}), f32[64,2,96]{2,1,0:T(2,128)S(1)}, u32[]{:S(2)}, u32[]{:S(2)}) %all-to-all-start.1) | async-done | bytes 49184 | tf_op jit(solution)/shard_map/all_to_all | solution.py:25
  46.9 1.0 fusion.35
  47.9 1.1 broadcast_in_dim.25
  49.0 5.6 %all-to-all-start.2 = ((bf16[8,32,2048]{2,1,0:T(8,128)(2,1)}), bf16[8,32,2048]{2,1,0:T(8,128)(2,1)S(1)}, u32[]{:S(2)}, u32[]{:S(2)}) async-start(bf16[8,32,2048]{2,1,0:T(8,128)(2,1)} %broadcast_in_dim.25), calls=%async_computation.2 | async-start | bytes 2097152 | tf_op jit(solution)/shard_map/all_to_all | solution.py:25
  54.8 14.8 %all-to-all-done.2 = bf16[8,32,2048]{2,1,0:T(8,128)(2,1)S(1)} async-done(((bf16[8,32,2048]{2,1,0:T(8,128)(2,1)}), bf16[8,32,2048]{2,1,0:T(8,128)(2,1)S(1)}, u32[]{:S(2)}, u32[]{:S(2)}) %all-to-all-start.2) | async-done | bytes 1048608 | tf_op jit(solution)/shard_map/all_to_all | solution.py:25
  71.7 3.0 stack.11
  74.6 5.8 %all-to-all-start.3 = ((bf16[64,256,128]{2,1,0:T(8,128)(2,1)}), bf16[64,256,128]{2,1,0:T(8,128)(2,1)}, u32[]{:S(2)}, u32[]{:S(2)}) async-start(bf16[64,256,128]{2,1,0:T(8,128)(2,1)} %stack.11), calls=%async_computation.3 | async-start | bytes 8388608 | tf_op jit(solution)/shard_map/all_to_all | solution.py:19
  82.7 160.6 %all_gather.6 = bf16[512,256]{1,0:T(8,128)(2,1)S(1)} all-gather(bf16[8,256]{1,0:T(8,128)(2,1)S(1)} %pad_maximum_fusion.5), channel_id=1, replica_groups=mesh['sp'=64,'tp'=8] {'sp'}, dimensions={0}, use_global_device_ids=true | all-gather | bytes 266240 | tf_op jit(solution)/shard_map/all_gather | solution.py:47
  246.2 4.8 %all-gather.2.cloned.1.call-done = bf16[16384,128]{0,1:T(8,128)(2,1)} async-done(((bf16[256,128]{0,1:T(8,128)(2,1)}), bf16[16384,128]{0,1:T(8,128)(2,1)}) %all-gather.2.cloned.1.call-update) | async-done | bytes 4194320 | tf_op jit(solution)/shard_map/all_gather | solution.py:198
  251.0 6.4 %copy.26 = bf16[16384,128]{1,0:T(8,128)(2,1)} copy(bf16[16384,128]{0,1:T(8,128)(2,1)} %all-gather.2.cloned.1.call-done) | data formatting | bytes 8388608 | tf_op jit(solution)/shard_map/while | solution.py:177
  257.4 78.1 %while.4 = (s32[]{:T(128)}, f32[1,256]{1,0:T(1,128)S(1)}, f32[1,256]{1,0:T(1,128)S(1)}, f32[256,1,128]{0,2,1:T(8,128)S(1)}, f32[1,256]{1,0:T(1,128)S(1)}, /*inde...) while((s32[]{:T(128)}, f32[1,256]{1,0:T(1,128)S(1)}, ...), condition=%wide.region_12.13_spmd, body=%wide.region_7.12_spmd.sunk | while | flops 205128704 | bytes 8488073 | solution.py:177
  257.4 1.0 dynamic-slice_bitcast_fusion.2
  259.6 1.3 fusion.140
  260.9 1.3 fusion.139
  262.3 1.0 dynamic-slice_bitcast_fusion.2
  264.5 1.3 fusion.140
  265.8 1.3 fusion.139
  267.2 1.0 dynamic-slice_bitcast_fusion.2
  269.3 1.3 fusion.140
  270.7 1.3 fusion.139
  272.1 1.0 dynamic-slice_bitcast_fusion.2
  274.2 1.3 fusion.140
  275.6 1.3 fusion.139
  276.9 1.0 dynamic-slice_bitcast_fusion.2
  279.1 1.3 fusion.140
  280.5 1.3 fusion.139
  281.8 1.0 dynamic-slice_bitcast_fusion.2
  284.0 1.3 fusion.140
  285.3 1.3 fusion.139
  286.7 1.0 dynamic-slice_bitcast_fusion.2
  288.9 1.3 fusion.140
  290.2 1.3 fusion.139
  291.6 1.0 dynamic-slice_bitcast_fusion.2
  293.8 1.3 fusion.140
  295.1 1.3 fusion.139
  296.5 1.0 dynamic-slice_bitcast_fusion.2
  298.7 1.3 fusion.140
  300.0 1.3 fusion.139
  301.4 1.0 dynamic-slice_bitcast_fusion.2
  303.5 1.3 fusion.140
  304.9 1.3 fusion.139
  306.2 1.0 dynamic-slice_bitcast_fusion.2
  308.4 1.3 fusion.140
  309.8 1.3 fusion.139
  311.1 1.0 dynamic-slice_bitcast_fusion.2
  313.3 1.3 fusion.140
  314.6 1.3 fusion.139
  316.0 1.0 dynamic-slice_bitcast_fusion.2
  318.2 1.3 fusion.140
  319.5 1.3 fusion.139
  320.9 1.0 dynamic-slice_bitcast_fusion.2
  323.1 1.3 fusion.140
  324.4 1.3 fusion.139
  325.8 1.0 dynamic-slice_bitcast_fusion.2
  328.0 1.3 fusion.140
  329.3 1.3 fusion.139
  332.8 1.3 fusion.140
  334.2 1.3 fusion.139
  336.2 25.0 %all_to_all.25 = bf16[8,32,2048]{2,1,0:T(8,128)(2,1)S(1)} all-to-all(bf16[8,32,2048]{2,1,0:T(8,128)(2,1)S(1)} %bitcast.183), channel_id=1, replica_groups=mesh['sp'=64,'tp'=8] {'tp'}, dimensions={0} | all-to-all | bytes 2097152 | tf_op jit(solution)/shard_map/all_to_all | solution.py:58
  (213 shorter events, 28.7 us)
Async XLA Ops:
  6.5 329.1 %copy-start = (bf16[128,2048]{1,0:T(8,128)(2,1)S(1)}, bf16[128,2048]{1,0:T(8,128)(2,1)}, u32[]{:S(2)}) copy-start(bf16[128,2048]{1,0:T(8,128)(2,1)} %param.29) | copy-start | bytes 1572868
  6.5 63.0 %copy-start.3 = (bf16[2048,64]{0,1:T(8,128)(2,1)S(1)}, bf16[2048,64]{0,1:T(8,128)(2,1)}, u32[]{:S(2)}) copy-start(bf16[2048,64]{0,1:T(8,128)(2,1)} %param.23) | copy-start | bytes 786436
  6.5 63.5 %copy-start.4 = (bf16[2048,64]{0,1:T(8,128)(2,1)S(1)}, bf16[2048,64]{0,1:T(8,128)(2,1)}, u32[]{:S(2)}) copy-start(bf16[2048,64]{0,1:T(8,128)(2,1)} %param.24) | copy-start | bytes 786436
  6.5 64.7 %copy-start.1 = (bf16[2048,128]{1,0:T(8,128)(2,1)S(1)}, bf16[2048,128]{1,0:T(8,128)(2,1)}, u32[]{:S(2)}) copy-start(bf16[2048,128]{1,0:T(8,128)(2,1)} %param.25) | copy-start | bytes 1572868
  8.2 14.7 %all-to-all-start = ((f32[8,2,96]{2,1,0:T(2,128)}), f32[8,2,96]{2,1,0:T(2,128)S(1)}, u32[]{:S(2)}, u32[]{:S(2)}) async-start(f32[8,2,96]{2,1,0:T(2,128)} %broadcast_in_dim.22), calls=%async_computation | async-start | bytes 16384 | tf_op jit(solution)/shard_map/all_to_all | solution.py:25
  23.6 23.1 %all-to-all-start.1 = ((f32[64,2,96]{2,1,0:T(2,128)}), f32[64,2,96]{2,1,0:T(2,128)S(1)}, u32[]{:S(2)}, u32[]{:S(2)}) async-start(f32[64,2,96]{2,1,0:T(2,128)} %broadcast_in_dim.23), calls=%async_computation.1 | async-start | bytes 131072 | tf_op jit(solution)/shard_map/all_to_all | solution.py:25
  49.0 20.6 %all-to-all-start.2 = ((bf16[8,32,2048]{2,1,0:T(8,128)(2,1)}), bf16[8,32,2048]{2,1,0:T(8,128)(2,1)S(1)}, u32[]{:S(2)}, u32[]{:S(2)}) async-start(bf16[8,32,2048]{2,1,0:T(8,128)(2,1)} %broadcast_in_dim.25), calls=%async_computation.2 | async-start | bytes 2097152 | tf_op jit(solution)/shard_map/all_to_all | solution.py:25
  54.6 196.4 %all-gather.2.cloned.1.call-start = ((), (), s32[]{:S(2)}) async-start(), calls=%async_computation.5 | async-start | bytes 4259840 | tf_op jit(solution)/shard_map/all_gather | solution.py:198
  74.6 7.1 %copy-start.7 = (bf16[8,2048]{1,0:T(8,128)(2,1)S(1)}, bf16[8,2048]{1,0:T(8,128)(2,1)}, u32[]{:S(2)}) copy-start(bf16[8,2048]{1,0:T(8,128)(2,1)} %param.17) | copy-start | bytes 98308
  74.6 168.7 %copy-start.5 = (bf16[2048,64]{0,1:T(8,128)(2,1)S(1)}, bf16[2048,64]{0,1:T(8,128)(2,1)}, u32[]{:S(2)}) copy-start(bf16[2048,64]{0,1:T(8,128)(2,1)} %param.22) | copy-start | bytes 786436
  74.6 169.2 %copy-start.6 = (bf16[2048,64]{0,1:T(8,128)(2,1)S(1)}, bf16[2048,64]{0,1:T(8,128)(2,1)}, u32[]{:S(2)}) copy-start(bf16[2048,64]{0,1:T(8,128)(2,1)} %param.21) | copy-start | bytes 786436
  74.6 182.8 %all-to-all-start.3 = ((bf16[64,256,128]{2,1,0:T(8,128)(2,1)}), bf16[64,256,128]{2,1,0:T(8,128)(2,1)}, u32[]{:S(2)}, u32[]{:S(2)}) async-start(bf16[64,256,128]{2,1,0:T(8,128)(2,1)} %stack.11), calls=%async_computation.3 | async-start | bytes 8388608 | tf_op jit(solution)/shard_map/all_to_all | solution.py:19
  257.4 78.2 %copy-start.8 = (f32[128]{0:T(128)S(1)}, f32[128]{0:T(128)}, u32[]{:S(2)}) copy-start(f32[128]{0:T(128)} %param.28) | copy-start | bytes 1540
  335.5 25.8 %copy-start.2 = (bf16[32,2048]{1,0:T(8,128)(2,1)S(1)}, bf16[32,2048]{1,0:T(8,128)(2,1)}, u32[]{:S(2)}) copy-start(bf16[32,2048]{1,0:T(8,128)(2,1)} %param.16) | copy-start | bytes 393220
Sparse Core Ops, SparseCore 0:
  71.3 179.6 all-gather.1
